TPU v7x, 256 devices: a whole 4x4x8 slice. The times are simulated.
256 devices in a mesh: ep: 16 (over y, x), tp: 16 (over z, core).
Axes of the slice: x: 4, y: 4, z: 8, core: 2. Of those that a mesh axis runs over, the one named last changes fastest.
Arguments:
- scan_source_values: bfloat16 [1024, 32768], P('tp', 'ep'), may hold values from -6 to 6
- switch_path_values: bfloat16 [1024, 32768], P('tp', 'ep'), may hold values from -6 to 6
- causal_filter_coefficients: bfloat16 [1024, 4], replicated, may hold values from -3 to 3
- scan_switch_blockmap: bfloat16 [16, 64, 64], replicated, may hold values from -0.75 to 0.75
- entry_switch_blockmap: bfloat16 [16, 64, 64], replicated, may hold values from -0.75 to 0.75
- feature_fading_speeds: float32 [1024], replicated, may hold values from 0 to 1
- spike_amount: float32 [32768], P('ep'), may hold values from -1 to 0
- final_linear_map: bfloat16 [1024, 2048], replicated, may hold values from -0.1875 to 0.1875
- dispatched_group_activity: bfloat16 [32768, 2048], P(('ep', 'tp')), may hold values from -6 to 6
- specialist_rmsgain: bfloat16 [2048], replicated, may hold values from 0.099609375 to 1.8984375
- selected_specialist_ids: int32 [32768, 2], P(('ep', 'tp')), may hold values from 0 to 15, all different within a row; in each aligned block of 128 rows (0 to 127, 128 to 255, ...) at most 24 rows name the same one
- selected_specialist_share: float32 [32768, 2], P(('ep', 'tp')), may hold values from 0.2 to 1
- specialist_switch_maps: bfloat16 [16, 2048, 2048], P('ep', None, 'tp'), may hold values from -0.3125 to 0.3125
- specialist_widen_maps: bfloat16 [16, 2048, 2048], P('ep', None, 'tp'), may hold values from -0.3125 to 0.3125
- specialist_shrink_maps: bfloat16 [16, 2048, 2048], P('ep', None, 'tp'), may hold values from -0.03125 to 0.03125
Outputs:
- scan_path_result: bfloat16 [32768, 2048], P(('ep', 'tp'))
- moe_out: bfloat16 [32768, 2048], P(('ep', 'tp'))
Inputs may be any that keep to these rules, and one draw needn't show every extreme that they name: `selected_specialist_ids`: each row names 2 different experts. Among the rows of one device no expert is named more than 24 times, and in every draw some device names some expert exactly 24 times.
All inputs are finite; a program needn't handle non-finite values.
Results may differ from a plain program's by a relative error of at most 0.0085.
Values may be sent and summed in bfloat16 or wider, within the bound.
A program may use at most 128 MiB of HBM per device.

v0:
```python
import jax
import jax.numpy as jnp
from jax import lax
from jax.sharding import PartitionSpec as P

BLOCK = 64


def from_everyone(x, axis):
    copies = jnp.broadcast_to(x, (lax.axis_size(axis), *x.shape))
    return lax.all_to_all(copies, axis, split_axis=0, concat_axis=0, tiled=True)


def all_in_one(x, axis):
    leaves = jax.tree.leaves(x)
    sequence = sorted(range(len(leaves)), key=lambda k: -leaves[k].size)
    width = (1, *leaves[sequence[0]].shape)[-1]
    lines = [
        jnp.pad(leaves[k].reshape(-1), (0, -leaves[k].size % width)).reshape(-1, width)
        for k in sequence
    ]
    both, at, found = (from_everyone(jnp.concatenate(lines), axis), 0, {})
    for k, line in zip(sequence, lines):
        section = both[:, at : at + len(line)].reshape(len(both), -1)
        found[k] = section[:, : leaves[k].size].reshape(-1, *leaves[k].shape)
        at += len(line)
    numbers = iter(range(len(leaves)))
    return jax.tree.map(lambda _: found[next(numbers)], x)


def folded_in_pairs(pieces, combine):
    while len(jax.tree.leaves(pieces)[0]) > 1:
        pieces = jax.vmap(combine)(
            *(jax.tree.map(lambda part: part[side::2], pieces) for side in (0, 1))
        )
    return jax.tree.map(lambda part: part[0], pieces)


def prefix(x, axis, combine, identity):
    count, index = (lax.axis_size(axis), lax.axis_index(axis))
    passed = jnp.arange(count) < index

    def kept(part, zero, own):
        part = jnp.where(
            passed.reshape(-1, *(1 for _ in own.shape)), part, jnp.asarray(zero, own.dtype)
        )
        return part

    pieces = all_in_one(x, axis)
    return folded_in_pairs(jax.tree.map(kept, pieces, identity, x), combine)


def from_behind(x, axis, by):
    count = lax.axis_size(axis)
    pairs = [(i, i + by) for i in range(count) if 0 <= i + by < count]
    return lax.ppermute(x, axis, pairs)


def cut_along(x, dim, count):
    dims = x.shape
    blocks = x.reshape(*dims[:dim], count, dims[dim] // count, *dims[dim + 1 :])
    return jnp.moveaxis(blocks, dim, 0)


def cut_rows(length, count):
    hop = length // count
    if hop >= 8:
        hop -= hop % 8
    return [hop * k for k in range(1, count)]


def laid_out(blocks, dim):
    blocks = jnp.moveaxis(blocks, 0, dim)
    dims = blocks.shape
    return blocks.reshape(*dims[:dim], dims[dim] * dims[dim + 1], *dims[dim + 2 :])


def cut_exchange(x, axis, pieces, split_dim, concat_dim):
    blocks = cut_along(x, split_dim, lax.axis_size(axis))
    split_at = max(range(1, max(2, blocks.ndim - 1)), key=lambda d: blocks.shape[d])
    finished = []
    for section in jnp.split(blocks, cut_rows(blocks.shape[split_at], pieces), axis=split_at):
        if section.size:
            finished.append(lax.all_to_all(section, axis, split_axis=0, concat_axis=0, tiled=True))
    return laid_out(jnp.concatenate(finished, axis=split_at), concat_dim)


def sent_together(arrays, axis, dim, along):
    ends, at = ([], 0)
    for a in arrays[:-1]:
        at += a.shape[along]
        ends.append(at)
    both = jnp.concatenate(arrays, axis=along)
    return tuple(jnp.split(lax.all_gather(both, axis, axis=dim, tiled=True), ends, axis=along))


def combine_pairs(earlier, later):
    return (earlier[0] * later[0], later[0] * earlier[1] + later[1])


def expert_units(rows, gate_piece, up_piece):
    gate_pre = jnp.dot(rows, gate_piece, preferred_element_type=jnp.float32)
    up_pre = jnp.dot(rows, up_piece, preferred_element_type=jnp.float32)
    gate_cut = jnp.minimum(gate_pre, 7.0)
    up_cut = jnp.clip(up_pre, -7.0, 7.0)
    return ((up_cut + 1.0) * gate_cut * jax.nn.sigmoid(1.702 * gate_cut)).astype(jnp.bfloat16)


def down_product(units, down_piece):
    return lax.dot_general(
        units, down_piece, (((1,), (1,)), ((), ())), preferred_element_type=jnp.float32
    )


def segment_recurrence(decay, drive):
    channels, positions = decay.shape
    span = 16
    seg_count = positions // span
    decay_split = decay.reshape(channels, seg_count, span).transpose(0, 2, 1)
    drive_split = drive.reshape(channels, seg_count, span).transpose(0, 2, 1)
    run_state = jnp.zeros((channels, seg_count), jnp.float32)
    run_decay = jnp.ones((channels, seg_count), jnp.float32)
    state_list = []
    decay_list = []
    for offset in range(span):
        run_state = decay_split[:, offset] * run_state + drive_split[:, offset]
        run_decay = run_decay * decay_split[:, offset]
        state_list.append(run_state)
        decay_list.append(run_decay)
    local_state = jnp.stack(state_list, axis=1)
    local_decay = jnp.stack(decay_list, axis=1)
    decay_upto, state_upto = lax.associative_scan(combine_pairs, (run_decay, run_state), axis=1)
    decay_before = jnp.concatenate(
        [jnp.ones((channels, 1), jnp.float32), decay_upto[:, :-1]], axis=1
    )
    state_before = jnp.concatenate(
        [jnp.zeros((channels, 1), jnp.float32), state_upto[:, :-1]], axis=1
    )
    identity = (jnp.ones((channels,), jnp.float32), jnp.zeros((channels,), jnp.float32))
    carried = prefix((decay_upto[:, -1], state_upto[:, -1]), "ep", combine_pairs, identity)
    entering = state_before + decay_before * carried[1][:, None]
    state = local_state + local_decay * entering[:, None, :]
    return state.transpose(0, 2, 1).reshape(channels, positions)


def mixer_half(
    scan_source_values,
    switch_path_values,
    causal_filter_coefficients,
    scan_switch_blockmap,
    entry_switch_blockmap,
    feature_fading_speeds,
    spike_amount,
    final_linear_map,
):
    channels, positions = scan_source_values.shape
    tp_index = lax.axis_index("tp")
    first_chan = tp_index * channels
    conv_local = lax.dynamic_slice_in_dim(
        causal_filter_coefficients, first_chan, channels, 0
    ).astype(jnp.float32)
    tap_count = conv_local.shape[1]
    rim_cells = from_behind(scan_source_values[:, positions - tap_count + 1 :], "ep", 1)
    padded = jnp.concatenate([rim_cells, scan_source_values], axis=1).astype(jnp.float32)
    running = padded[:, 0:positions] * conv_local[:, 0:1]
    for shift_tap in range(1, tap_count):
        running = (
            running
            + padded[:, shift_tap : shift_tap + positions]
            * conv_local[:, shift_tap : shift_tap + 1]
        )
    conv_out = running.astype(jnp.bfloat16)
    block_count = channels // BLOCK
    rate_local = lax.dynamic_slice_in_dim(
        scan_switch_blockmap, tp_index * block_count, block_count, 0
    )
    input_local = lax.dynamic_slice_in_dim(
        entry_switch_blockmap, tp_index * block_count, block_count, 0
    )
    grouped = conv_out.reshape(block_count, BLOCK, positions)
    block_dims = (((1,), (1,)), ((0,), (0,)))
    scan_switch = jax.nn.sigmoid(
        lax.dot_general(
            rate_local, grouped, block_dims, preferred_element_type=jnp.float32
        ).reshape(channels, positions)
    )
    inflow = jax.nn.sigmoid(
        lax.dot_general(
            input_local, grouped, block_dims, preferred_element_type=jnp.float32
        ).reshape(channels, positions)
    )
    feature_fading = lax.dynamic_slice_in_dim(feature_fading_speeds, first_chan, channels, 0)
    fading_exponent = -8.0 * scan_switch * feature_fading[:, None] + spike_amount[None, :]
    drive = jnp.sqrt(-jnp.expm1(2.0 * fading_exponent)) * inflow * conv_out.astype(jnp.float32)
    state = segment_recurrence(jnp.exp(fading_exponent), drive)
    mix_hidden = (
        state * jax.nn.gelu(switch_path_values.astype(jnp.float32), approximate=True)
    ).astype(jnp.bfloat16)
    tp_count = lax.axis_size("tp")
    pieces = mix_hidden.reshape(channels, tp_count, positions // tp_count)
    return lax.dot_general(
        lax.all_to_all(pieces, "tp", split_axis=1, concat_axis=0, tiled=True)[:, 0, :],
        final_linear_map,
        (((0,), (0,)), ((), ())),
        preferred_element_type=jnp.float32,
    ).astype(jnp.bfloat16)


def expert_half(
    dispatched_group_activity,
    specialist_rmsgain,
    selected_specialist_ids,
    selected_specialist_share,
    specialist_switch_maps,
    specialist_widen_maps,
    specialist_shrink_maps,
):
    token_count, model_width = dispatched_group_activity.shape
    route_count = selected_specialist_ids.shape[1]
    expert_count = lax.axis_size("ep")
    slot_count = 3 * route_count * token_count // (2 * expert_count)
    values = dispatched_group_activity.astype(jnp.float32)
    scale = lax.rsqrt(jnp.mean(values * values, axis=1, keepdims=True) + 1e-06)
    normed = (values * scale * specialist_rmsgain.astype(jnp.float32)).astype(jnp.bfloat16)
    flat_ids = selected_specialist_ids.reshape(-1)
    one_hot = (flat_ids[:, None] == jnp.arange(expert_count, dtype=jnp.int32)[None, :]).astype(
        jnp.int32
    )
    slot_rank = jnp.sum((jnp.cumsum(one_hot, axis=0) - one_hot) * one_hot, axis=1)
    slot_place = flat_ids * slot_count + slot_rank
    owner_token = jnp.arange(token_count * route_count, dtype=jnp.int32) // route_count
    slot_token = (
        jnp.full((expert_count * slot_count,), token_count, jnp.int32)
        .at[slot_place]
        .set(owner_token)
    )
    padded_rows = jnp.concatenate([normed, jnp.zeros((1, model_width), jnp.bfloat16)], axis=0)
    outgoing = padded_rows[slot_token].reshape(expert_count, slot_count, model_width)
    arrived = cut_exchange(outgoing, "ep", 2, 0, 0).reshape(expert_count * slot_count, model_width)
    gate_shard = specialist_switch_maps[0]
    up_shard = specialist_widen_maps[0]
    down_shard = specialist_shrink_maps[0]
    gate_full, up_full, down_full = sent_together((gate_shard, up_shard, down_shard), "tp", 1, 0)
    result = down_product(expert_units(arrived, gate_full, up_full), down_full)
    outbound = result.astype(jnp.bfloat16).reshape(expert_count, slot_count, model_width)
    returned = lax.all_to_all(outbound, "ep", split_axis=0, concat_axis=0, tiled=True).reshape(
        expert_count * slot_count, model_width
    )
    chosen = returned[slot_place].reshape(token_count, route_count, model_width).astype(jnp.float32)
    return jnp.sum(chosen * selected_specialist_share[:, :, None], axis=1).astype(jnp.bfloat16)


def on_device(
    scan_source_values,
    switch_path_values,
    causal_filter_coefficients,
    scan_switch_blockmap,
    entry_switch_blockmap,
    feature_fading_speeds,
    spike_amount,
    final_linear_map,
    dispatched_group_activity,
    specialist_rmsgain,
    selected_specialist_ids,
    selected_specialist_share,
    specialist_switch_maps,
    specialist_widen_maps,
    specialist_shrink_maps,
):
    scan_path_result = mixer_half(
        scan_source_values,
        switch_path_values,
        causal_filter_coefficients,
        scan_switch_blockmap,
        entry_switch_blockmap,
        feature_fading_speeds,
        spike_amount,
        final_linear_map,
    )
    moe_out = expert_half(
        dispatched_group_activity,
        specialist_rmsgain,
        selected_specialist_ids,
        selected_specialist_share,
        specialist_switch_maps,
        specialist_widen_maps,
        specialist_shrink_maps,
    )
    return (scan_path_result, moe_out)


def solution(mesh):
    in_specs = (
        P("tp", "ep"),
        P("tp", "ep"),
        P(),
        P(),
        P(),
        P(),
        P("ep"),
        P(),
        P(("ep", "tp"), None),
        P(),
        P(("ep", "tp"), None),
        P(("ep", "tp"), None),
        P("ep", None, "tp"),
        P("ep", None, "tp"),
        P("ep", None, "tp"),
    )
    out_specs = (P(("ep", "tp"), None), P(("ep", "tp"), None))
    return jax.shard_map(
        on_device, mesh=mesh, in_specs=in_specs, out_specs=out_specs, check_vma=False
    )
```

profile of v0, /device:TPU:1, one launch (start us, length us, event | category | flops | bytes accessed | tf_op | source)
XLA Modules:
  0.0 230.1 jit_solution(9406618166542396886)
XLA Ops:
  7.3 2.7 %pad_maximum_fusion.1 = bf16[6144,128]{1,0:T(8,128)(2,1)} fusion(bf16[2048,128]{1,0:T(8,128)(2,1)} %bitcast.310, bf16[2048,128]{1,0:T(8,128)(2,1)} %bitcast.311, bf16[2048,128]{1,0:T(8,128)(2,1)} %bitcast.312), kind=kLoop, calls=%fused_computation.24 | loop fusion | flops 4718592 | bytes 3145728 | tf_op jit(solution)/shard_map/concatenate | solution.py:93
  10.1 3.9 %collective-permute-start = (bf16[64,3]{1,0:T(8,128)(2,1)S(1)}, bf16[64,3]{1,0:T(8,128)(2,1)S(1)}, u32[]{:S(2)}, u32[]{:S(2)}) collective-permute-start(bf16[64,3]{1,0:T(8,128)(2,1)S(1)} %slice.411), channel_id=1, source_target_pairs={{0,16},{16,32},{32,48},{48,64},{64,80},{80,96},{96,112},{112,128},... | collective-permute-start | bytes 1160 | tf_op jit(solution)/shard_map/ppermute | solution.py:56
  14.1 0.1 eq.29
  14.3 0.1 eq.25
  14.5 0.6 reduce-window.6
  15.0 0.2 slice_reduce_fusion
  15.4 0.1 mul.822
  15.6 0.2 fusion.25
  15.8 0.2 fusion.27
  16.1 1.4 scatter_custom_fusion
  17.6 2.5 %gather_fusion = bf16[384,2048]{1,0:T(8,128)(2,1)S(1)} fusion(bf16[129,2048]{1,0:T(8,128)(2,1)S(1)} %concatenate.73, s32[1024]{0:T(1024)S(1)} %pad_clamp_fusion.1), kind=kCustom, calls=%fused_computation | custom fusion | bytes 3147264 | tf_op jit(solution)/shard_map/gather | solution.py:238
  20.0 0.8 dynamic-slice_multiply_fusion
  20.8 0.7 dynamic-slice_convert_fusion
  21.6 1.0 split.21
  22.6 0.8 split.20
  23.5 0.1 maximum_convert_fusion
  23.7 0.5 fusion.36
  24.2 0.3 fusion.20
  24.5 0.3 copy.49
  24.9 0.3 exponential_bitcast_fusion
  25.2 0.9 fusion.74
  26.3 1.3 fusion.17
  27.6 0.3 copy.51
  27.9 0.3 copy.101
  28.2 0.1 bitcast_add_fusion
  29.9 0.7 reshape.178
  30.6 6.5 %all-to-all-start = ((f32[16,1,128]{2,1,0:T(1,128)}), f32[16,1,128]{2,1,0:T(1,128)S(1)}, u32[]{:S(2)}, u32[]{:S(2)}) async-start(f32[16,1,128]{2,1,0:T(1,128)} %reshape.178), calls=%async_computation | async-start | bytes 16384 | tf_op jit(solution)/shard_map/all_to_all | solution.py:11
  37.1 0.6 constant_dynamic-update-slice_fusion.31
  37.8 0.6 constant_dynamic-update-slice_fusion.30
  38.4 0.6 constant_dynamic-update-slice_fusion.29
  39.0 0.6 constant_dynamic-update-slice_fusion.28
  39.7 0.6 constant_dynamic-update-slice_fusion.27
  40.3 0.6 constant_dynamic-update-slice_fusion.26
  41.0 0.6 constant_dynamic-update-slice_fusion.25
  41.6 0.6 constant_dynamic-update-slice_fusion.24
  42.2 0.6 constant_dynamic-update-slice_fusion.23
  42.9 0.6 constant_dynamic-update-slice_fusion.22
  43.5 0.6 constant_dynamic-update-slice_fusion.21
  44.2 0.6 constant_dynamic-update-slice_fusion.20
  44.8 0.6 constant_dynamic-update-slice_fusion.19
  45.4 0.7 constant_dynamic-update-slice_fusion.18
  46.1 0.6 constant_dynamic-update-slice_fusion.17
  46.7 0.6 constant_dynamic-update-slice_fusion.16
  47.4 6.7 %all-to-all-start.2 = ((bf16[16,1,8,2048]{3,2,1,0:T(8,128)(2,1)}), bf16[16,1,8,2048]{3,2,1,0:T(8,128)(2,1)S(1)}, u32[]{:S(2)}, u32[]{:S(2)}) async-start(bf16[16,1,8,2048]{3,2,1,0:T(8,128)(2,1)} %split.20), calls=%async_computation.2 | async-start | bytes 1048576 | tf_op jit(solution)/shard_map/all_to_all | solution.py:84
  54.0 0.5 broadcast.206
  54.6 0.7 reduce.2
  55.7 8.4 %all-to-all-done.2 = bf16[16,1,8,2048]{3,2,1,0:T(8,128)(2,1)S(1)} async-done(((bf16[16,1,8,2048]{3,2,1,0:T(8,128)(2,1)}), bf16[16,1,8,2048]{3,2,1,0:T(8,128)(2,1)S(1)}, u32[]{:S(2)}, u32[]{:S(2)}) %all-to-all-start.2) | async-done | bytes 524320 | tf_op jit(solution)/shard_map/all_to_all | solution.py:84
  64.1 3.7 %all-to-all-start.3 = ((bf16[16,1,16,2048]{3,2,1,0:T(8,128)(2,1)}), bf16[16,1,16,2048]{3,2,1,0:T(8,128)(2,1)S(1)}, u32[]{:S(2)}, u32[]{:S(2)}) async-start(bf16[16,1,16,2048]{3,2,1,0:T(8,128)(2,1)} %split.21), calls=%async_computation.3 | async-start | bytes 2097152 | tf_op jit(solution)/shard_map/all_to_all | solution.py:84
  67.8 1.4 add_bitcast_fusion
  69.2 0.6 copy.70
  69.9 0.3 copy.71
  70.2 0.9 copy_bitcast_fusion.1
  71.1 11.6 %all-to-all-done.3 = bf16[16,1,16,2048]{3,2,1,0:T(8,128)(2,1)S(1)} async-done(((bf16[16,1,16,2048]{3,2,1,0:T(8,128)(2,1)}), bf16[16,1,16,2048]{3,2,1,0:T(8,128)(2,1)S(1)}, u32[]{:S(2)}, u32[]{:S(2)}) %all-to-all-start.3) | async-done | bytes 1048608 | tf_op jit(solution)/shard_map/all_to_all | solution.py:84
  82.7 12.0 %all-to-all-start.1 = ((bf16[64,16,128]{2,0,1:T(8,128)(2,1)}), bf16[64,16,128]{2,0,1:T(8,128)(2,1)S(1)}, u32[]{:S(2)}, u32[]{:S(2)}) async-start(bf16[64,16,128]{2,0,1:T(8,128)(2,1)} %copy_bitcast_fusion.1), calls=%async_computation.1 | async-start | bytes 524288 | tf_op jit(solution)/shard_map/all_to_all | solution.py:202
  94.7 0.2 pad_maximum_fusion
  94.9 66.8 %all-gather.2.cloned.1.call-done = bf16[6144,2048]{1,0:T(8,128)(2,1)} async-done(((bf16[6144,128]{1,0:T(8,128)(2,1)}), bf16[6144,2048]{1,0:T(8,128)(2,1)}) %all-gather.2.cloned.1.call-update) | async-done | bytes 25165840 | tf_op jit(solution)/shard_map/all_gather | solution.py:94
  161.7 8.4 %fusion.2 = f32[384,2048]{1,0:T(8,128)} fusion(bf16[384,2048]{1,0:T(8,128)(2,1)S(1)} %bitcast.289, bf16[6144,2048]{1,0:T(8,128)(2,1)} %all-gather.2.cloned.1.call-done), kind=kOutput, calls=%fused_computation.5 | convolution fusion | flops 3221225472 | bytes 13107200 | tf_op jit(solution)/shard_map/dot_general | solution.py:102
  170.1 15.3 %fusion.8 = bf16[384,2048]{1,0:T(8,128)(2,1)} fusion(bf16[6144,2048]{1,0:T(8,128)(2,1)} %all-gather.2.cloned.1.call-done, f32[384,2048]{1,0:T(8,128)} %fusion.2, bf16[384,2048]{1,0:T(8,128)(2,1)S(1)} %bitcast.290), kind=kOutput, calls=%fused_computation.10 | convolution fusion | flops 6451101696 | bytes 23068672 | tf_op jit(solution)/shard_map/dot_general | solution.py:110
  185.4 6.7 %all-to-all-start.4 = ((bf16[16,24,2048]{2,1,0:T(8,128)(2,1)}), bf16[16,24,2048]{2,1,0:T(8,128)(2,1)S(1)}, u32[]{:S(2)}, u32[]{:S(2)}) async-start(bf16[16,24,2048]{2,1,0:T(8,128)(2,1)} %bitcast.64), calls=%async_computation.4 | async-start | bytes 3145728 | tf_op jit(solution)/shard_map/all_to_all | solution.py:246
  192.2 3.7 %convolution_convert_fusion = bf16[128,2048]{1,0:T(8,128)(2,1)} fusion(bf16[1024,128]{1,0:T(8,128)(2,1)S(1)} %bitcast.306, bf16[1024,2048]{1,0:T(8,128)(2,1)} %param.22), kind=kOutput, calls=%fused_computation.11 | convolution fusion | flops 537133056 | bytes 4980736 | tf_op jit(solution)/shard_map/dot_general | solution.py:201
  195.9 20.7 %all-to-all-done.4 = bf16[16,24,2048]{2,1,0:T(8,128)(2,1)S(1)} async-done(((bf16[16,24,2048]{2,1,0:T(8,128)(2,1)}), bf16[16,24,2048]{2,1,0:T(8,128)(2,1)S(1)}, u32[]{:S(2)}, u32[]{:S(2)}) %all-to-all-start.4) | async-done | bytes 1572896 | tf_op jit(solution)/shard_map/all_to_all | solution.py:246
  216.6 1.4 gather_fusion.1
  218.0 1.3 reshape.149
  219.4 3.9 %multiply_reduce_fusion = bf16[128,2048]{1,0:T(8,128)(2,1)} fusion(f32[128,2,2048]{2,1,0:T(2,128)S(1)} %reshape.149, f32[128,2]{1,0:T(8,128)S(1)} %copy.79), kind=kLoop, calls=%fused_computation.22 | loop fusion | flops 786432 | bytes 2622464 | tf_op jit(solution)/shard_map/reduce_sum | solution.py:250
  (177 shorter events, 2.6 us)
Async XLA Ops:
  7.2 17.0 %copy-start = (bf16[16,64,64]{2,1,0:T(8,128)(2,1)S(1)}, bf16[16,64,64]{2,1,0:T(8,128)(2,1)}, u32[]{:S(2)}) copy-start(bf16[16,64,64]{2,1,0:T(8,128)(2,1)} %param.18) | copy-start | bytes 393220
  7.2 2.8 %copy-start.3 = (bf16[64,2048]{1,0:T(8,128)(2,1)S(1)}, bf16[64,2048]{1,0:T(8,128)(2,1)}, u32[]{:S(2)}) copy-start(bf16[64,2048]{1,0:T(8,128)(2,1)} %param.15) | copy-start | bytes 786436
  7.2 6.8 %copy-start.6 = (s32[128,2]{0,1:T(2,128)S(1)}, s32[128,2]{0,1:T(2,128)}, u32[]{:S(2)}) copy-start(s32[128,2]{0,1:T(2,128)} %param.25) | copy-start | bytes 3076
  7.2 8.3 %copy-start.7 = (bf16[2048]{0:T(1024)(128)(2,1)S(1)}, bf16[2048]{0:T(1024)(128)(2,1)}, u32[]{:S(2)}) copy-start(bf16[2048]{0:T(1024)(128)(2,1)} %param.24) | copy-start | bytes 12292
  7.2 8.3 %copy-start.2 = (bf16[128,2048]{1,0:T(8,128)(2,1)S(1)}, bf16[128,2048]{1,0:T(8,128)(2,1)}, u32[]{:S(2)}) copy-start(bf16[128,2048]{1,0:T(8,128)(2,1)} %param.23) | copy-start | bytes 1572868
  7.2 154.4 %all-gather.2.cloned.1.call-start = ((), (), s32[]{:S(2)}) async-start(), calls=%async_computation.5 | async-start | bytes 26738688 | tf_op jit(solution)/shard_map/all_gather | solution.py:94
  10.1 13.4 %collective-permute-start = (bf16[64,3]{1,0:T(8,128)(2,1)S(1)}, bf16[64,3]{1,0:T(8,128)(2,1)S(1)}, u32[]{:S(2)}, u32[]{:S(2)}) collective-permute-start(bf16[64,3]{1,0:T(8,128)(2,1)S(1)} %slice.411), channel_id=1, source_target_pairs={{0,16},{16,32},{32,48},{48,64},{64,80},{80,96},{96,112},{112,128},... | collective-permute-start | bytes 1160 | tf_op jit(solution)/shard_map/ppermute | solution.py:56
  20.0 3.4 %copy-start.5 = (f32[2048]{0:T(1024)S(1)}, f32[2048]{0:T(1024)}, u32[]{:S(2)}) copy-start(f32[2048]{0:T(1024)} %param.21) | copy-start | bytes 24580
  30.6 16.8 %all-to-all-start = ((f32[16,1,128]{2,1,0:T(1,128)}), f32[16,1,128]{2,1,0:T(1,128)S(1)}, u32[]{:S(2)}, u32[]{:S(2)}) async-start(f32[16,1,128]{2,1,0:T(1,128)} %reshape.178), calls=%async_computation | async-start | bytes 16384 | tf_op jit(solution)/shard_map/all_to_all | solution.py:11
  47.4 16.7 %all-to-all-start.2 = ((bf16[16,1,8,2048]{3,2,1,0:T(8,128)(2,1)}), bf16[16,1,8,2048]{3,2,1,0:T(8,128)(2,1)S(1)}, u32[]{:S(2)}, u32[]{:S(2)}) async-start(bf16[16,1,8,2048]{3,2,1,0:T(8,128)(2,1)} %split.20), calls=%async_computation.2 | async-start | bytes 1048576 | tf_op jit(solution)/shard_map/all_to_all | solution.py:84
  64.1 18.6 %all-to-all-start.3 = ((bf16[16,1,16,2048]{3,2,1,0:T(8,128)(2,1)}), bf16[16,1,16,2048]{3,2,1,0:T(8,128)(2,1)S(1)}, u32[]{:S(2)}, u32[]{:S(2)}) async-start(bf16[16,1,16,2048]{3,2,1,0:T(8,128)(2,1)} %split.21), calls=%async_computation.3 | async-start | bytes 2097152 | tf_op jit(solution)/shard_map/all_to_all | solution.py:84
  67.8 2.4 %copy-start.4 = (bf16[64,2048]{1,0:T(8,128)(2,1)S(1)}, bf16[64,2048]{1,0:T(8,128)(2,1)}, u32[]{:S(2)}) copy-start(bf16[64,2048]{1,0:T(8,128)(2,1)} %param.16) | copy-start | bytes 786436
  82.7 102.7 %all-to-all-start.1 = ((bf16[64,16,128]{2,0,1:T(8,128)(2,1)}), bf16[64,16,128]{2,0,1:T(8,128)(2,1)S(1)}, u32[]{:S(2)}, u32[]{:S(2)}) async-start(bf16[64,16,128]{2,0,1:T(8,128)(2,1)} %copy_bitcast_fusion.1), calls=%async_computation.1 | async-start | bytes 524288 | tf_op jit(solution)/shard_map/all_to_all | solution.py:202
  185.4 6.7 %copy-start.8 = (f32[128,2]{0,1:T(2,128)S(1)}, f32[128,2]{0,1:T(2,128)}, u32[]{:S(2)}) copy-start(f32[128,2]{0,1:T(2,128)} %param.26) | copy-start | bytes 3076
  185.4 31.2 %all-to-all-start.4 = ((bf16[16,24,2048]{2,1,0:T(8,128)(2,1)}), bf16[16,24,2048]{2,1,0:T(8,128)(2,1)S(1)}, u32[]{:S(2)}, u32[]{:S(2)}) async-start(bf16[16,24,2048]{2,1,0:T(8,128)(2,1)} %bitcast.64), calls=%async_computation.4 | async-start | bytes 3145728 | tf_op jit(solution)/shard_map/all_to_all | solution.py:246
  216.6 6.6 %copy-start.1 = (bf16[16,64,64]{2,1,0:T(8,128)(2,1)S(1)}, bf16[16,64,64]{2,1,0:T(8,128)(2,1)}, u32[]{:S(2)}) copy-start(bf16[16,64,64]{2,1,0:T(8,128)(2,1)} %param.18) | copy-start | bytes 393220
Sparse Core Ops, SparseCore 0:
  10.1 151.4 all-gather.1
where the time goes:
time: 231 us; the launch traced here: 230 us
  waiting for transfers between devices  108 us (47%)
  starting transfers between devices  39.4 us (17%)
  matrix products  29.1 us (13%)
  other arithmetic  23.6 us (10%)
  local copies, waits for them, and re-layouts  15.4 us (7%)
  between operations  15 us (6%)
    all_gather x1, waiting for transfers between devices, sent_together(): lax.all_gather(both, axis, axis=dim, tiled=True)  66.8 us
    all_to_all x1, waiting for transfers between devices, expert_half(): lax.all_to_all(outbound, 'ep', split_axis=0, concat_axis=0, tiled=True)  20.7 us
    all_to_all x2, waiting for transfers between devices, cut_exchange(): lax.all_to_all(section, axis, split_axis=0, concat_axis=0, tiled=True)  20 us
    dot_general x1, matrix products, down_product(): lax.dot_general(units, down_piece, (((1,), (1,)), ((), ())), preferred_el...  15.3 us
    all_to_all x1, starting transfers between devices, mixer_half(): lax.all_to_all(pieces, 'tp', split_axis=1, concat_axis=0, tiled=True)  12 us
    all_to_all x2, starting transfers between devices, cut_exchange(): lax.all_to_all(section, axis, split_axis=0, concat_axis=0, tiled=True)  10.3 us
    unnamed x16, other arithmetic  8.93 us
    dot_general x1, matrix products, expert_units(): gate_pre = jnp.dot(rows, gate_piece, preferred_element_type=jnp.float32)  8.43 us
  transfers between devices with their start and end apart: 7, of which 4 were waited for; matrix products, arithmetic and copies ran while one was open for 26% of the time, Pallas kernels for 0%

commit v1 on v0

--- a/solution.py
+++ b/solution.py
@@ -1,8 +1,25 @@
+import functools
+
 import jax
 import jax.numpy as jnp
 from jax import lax
+from jax.experimental import pallas as pl
+from jax.experimental.pallas import tpu as pltpu
 from jax.sharding import PartitionSpec as P
 
+MESH = pl.DeviceIdType.MESH
+F32 = jnp.float32
+BF16 = jnp.bfloat16
+CAP = 24
+ROWS = 384
+DM = 2048
+SHARD = 128
+NZ = 8
+NEP = 16
+NDC = 4
+DC = DM // NDC
+NG = 4
+GROWS = 1024
 BLOCK = 64
 
 
@@ -85,31 +102,8 @@
     return laid_out(jnp.concatenate(finished, axis=split_at), concat_dim)
 
 
-def sent_together(arrays, axis, dim, along):
-    ends, at = ([], 0)
-    for a in arrays[:-1]:
-        at += a.shape[along]
-        ends.append(at)
-    both = jnp.concatenate(arrays, axis=along)
-    return tuple(jnp.split(lax.all_gather(both, axis, axis=dim, tiled=True), ends, axis=along))
-
-
 def combine_pairs(earlier, later):
     return (earlier[0] * later[0], later[0] * earlier[1] + later[1])
-
-
-def expert_units(rows, gate_piece, up_piece):
-    gate_pre = jnp.dot(rows, gate_piece, preferred_element_type=jnp.float32)
-    up_pre = jnp.dot(rows, up_piece, preferred_element_type=jnp.float32)
-    gate_cut = jnp.minimum(gate_pre, 7.0)
-    up_cut = jnp.clip(up_pre, -7.0, 7.0)
-    return ((up_cut + 1.0) * gate_cut * jax.nn.sigmoid(1.702 * gate_cut)).astype(jnp.bfloat16)
-
-
-def down_product(units, down_piece):
-    return lax.dot_general(
-        units, down_piece, (((1,), (1,)), ((), ())), preferred_element_type=jnp.float32
-    )
 
 
 def segment_recurrence(decay, drive):
@@ -206,6 +200,254 @@
     ).astype(jnp.bfloat16)
 
 
+def expert_kernel(
+    tok_ref, gain_ref, meta_ref, g_ref, u_ref, d_ref, out_ref,
+    gbuf, ubuf, dbuf, snd, xin, xmat, units, acc, ps, pr, rs, rb, comb,
+    ag_send, ag_recv, ds_send, ds_recv, xs_send, xs_recv, ps_send, ps_recv, rt_send, rt_recv,
+):
+    ep = lax.axis_index("ep")
+    tp = lax.axis_index("tp")
+    z = tp // 2
+    core = lax.rem(tp, 2)
+    sib = z * 2 + (1 - core)
+    nbr = (lax.rem(z + 1, NZ) * 2 + core, lax.rem(z + NZ - 1, NZ) * 2 + core)
+
+    bar = pltpu.get_barrier_semaphore()
+    for who in (nbr[0], nbr[1], sib):
+        pl.semaphore_signal(bar, inc=1, device_id=(ep, who), device_id_type=MESH)
+
+    @pl.loop(1, NEP)
+    def _(k):
+        pl.semaphore_signal(bar, inc=1, device_id=(lax.rem(ep + k, NEP), tp), device_id_type=MESH)
+
+    pl.semaphore_wait(bar, 3 + NEP - 1)
+
+    def piece(p):
+        if p < NG:
+            return (g_ref, gbuf, (p % 2) * GROWS, GROWS) if p < 2 else (u_ref, ubuf, (p % 2) * GROWS, GROWS)
+        return d_ref, dbuf, (p - NG) * DC, DC
+
+    def ring(d, hop, p, origin):
+        own, buf, lo, n = piece(p)
+        last = isinstance(hop, int) and hop == 4
+        if last:
+            n = n // 2
+            lo = lo + d * n
+        first = isinstance(hop, int) and hop == 1
+        src = own.at[pl.ds(lo, n)] if first else buf.at[origin, pl.ds(lo, n)]
+        return pltpu.make_async_remote_copy(
+            src_ref=src, dst_ref=buf.at[origin, pl.ds(lo, n)],
+            send_sem=ag_send.at[d, hop - 1, p], recv_sem=ag_recv.at[d, hop - 1, p],
+            device_id=(ep, nbr[d]), device_id_type=MESH,
+        )
+
+    def sent(d, hop):
+        return lax.rem(z + NZ - (hop - 1), NZ) if d == 0 else lax.rem(z + hop - 1, NZ)
+
+    def came(d, hop):
+        return lax.rem(z + NZ - hop, NZ) if d == 0 else lax.rem(z + hop, NZ)
+
+    def start(pieces, hop):
+        for p in pieces:
+            for d in (0, 1):
+                ring(d, hop, p, sent(d, hop)).start()
+
+    def forward(pieces, hop, last=False):
+        for p in pieces:
+            for d in (0, 1):
+                ring(d, hop, p, came(d, hop)).wait_recv()
+                nxt = 4 if last else hop + 1
+                ring(d, nxt, p, sent(d, nxt)).start()
+
+    def arrive(pieces):
+        for p in pieces:
+            for d in (0, 1):
+                ring(d, 4, p, came(d, 4)).wait_recv()
+
+    gu = list(range(NG))
+    dn = list(range(NG, NG + NDC))
+    start(gu, 1)
+
+    gbuf[z] = g_ref[...]
+    ubuf[z] = u_ref[...]
+    dbuf[z] = d_ref[...]
+
+    values = tok_ref[...].astype(F32)
+    scale = lax.rsqrt(jnp.mean(values * values, axis=1, keepdims=True) + 1e-06)
+    normed = (values * scale * gain_ref[...].astype(F32)).astype(BF16)
+    expert_no = lax.broadcasted_iota(jnp.int32, (NEP, SHARD), 0).astype(F32)
+    is0 = meta_ref[0:1, :] == expert_no
+    is1 = meta_ref[1:2, :] == expert_no
+    member = jnp.where(is0 | is1, 1.0, 0.0)
+    weight = jnp.where(is0, meta_ref[2:3, :], 0.0) + jnp.where(is1, meta_ref[3:4, :], 0.0)
+    before = (
+        lax.broadcasted_iota(jnp.int32, (SHARD, SHARD), 0)
+        < lax.broadcasted_iota(jnp.int32, (SHARD, SHARD), 1)
+    )
+    rank = jnp.dot(
+        member.astype(BF16), jnp.where(before, 1.0, 0.0).astype(BF16), preferred_element_type=F32
+    )
+    place = jnp.where(member > 0.0, rank, -1.0)
+    slot_no = lax.broadcasted_iota(jnp.int32, (CAP, SHARD), 0).astype(F32)
+    picks, shares = [], []
+    for e in range(NEP):
+        hit = place[e : e + 1, :] == slot_no
+        picks.append(jnp.where(hit, 1.0, 0.0))
+        shares.append(jnp.where(hit, weight[e : e + 1, :], 0.0))
+    pick = jnp.concatenate(picks, axis=0).astype(BF16)
+    share = jnp.concatenate(shares, axis=0).T
+    share_hi = share.astype(BF16)
+    comb[0] = share_hi
+    comb[1] = (share - share_hi.astype(F32)).astype(BF16)
+    for k in range(4):
+        rows = jnp.dot(pick, normed[:, k * 512 : (k + 1) * 512], preferred_element_type=F32)
+        snd[:, :, k * 512 : (k + 1) * 512] = rows.reshape(NEP, CAP, 512).astype(BF16)
+
+    def dispatch(peer, src):
+        return pltpu.make_async_remote_copy(
+            src_ref=snd.at[peer], dst_ref=xin.at[core, src],
+            send_sem=ds_send.at[peer], recv_sem=ds_recv.at[src],
+            device_id=(peer, tp), device_id_type=MESH,
+        )
+
+    @pl.loop(1, NEP)
+    def _(k):
+        dispatch(lax.rem(ep + k, NEP), ep).start()
+
+    xin[core, ep] = snd[ep]
+
+    forward(gu, 1)
+
+    @pl.loop(1, NEP)
+    def _(k):
+        src = lax.rem(ep + k, NEP)
+        dispatch(src, src).wait_recv()
+
+    to_sib = pltpu.make_async_remote_copy(
+        src_ref=xin.at[core], dst_ref=xin.at[core], send_sem=xs_send, recv_sem=xs_recv,
+        device_id=(ep, sib), device_id_type=MESH,
+    )
+    from_sib = pltpu.make_async_remote_copy(
+        src_ref=xin.at[1 - core], dst_ref=xin.at[1 - core], send_sem=xs_send, recv_sem=xs_recv,
+        device_id=(ep, sib), device_id_type=MESH,
+    )
+    to_sib.start()
+    from_sib.wait_recv()
+
+    @pl.loop(0, 2 * (NEP // 2))
+    def _(i):
+        half = i // (NEP // 2)
+        pair = lax.rem(i, NEP // 2)
+        two = xin[half, pl.ds(pair * 2, 2)].astype(F32).reshape(2 * CAP, DM)
+        xmat[half, pl.ds(pl.multiple_of(pair * 2 * CAP, 16), 2 * CAP), :] = two.astype(BF16)
+
+    def hidden(origin):
+        @pl.loop(0, 2)
+        def _(half):
+            both = jnp.concatenate([gbuf[origin], ubuf[origin]], axis=1)
+            pre = jnp.dot(xmat[half], both, preferred_element_type=F32)
+            gate = jnp.minimum(pre[:, :SHARD], 7.0)
+            up = jnp.clip(pre[:, SHARD:], -7.0, 7.0)
+            units[half, origin] = ((up + 1.0) * gate * jax.nn.sigmoid(1.702 * gate)).astype(BF16)
+
+    def hidden_pair(hop):
+        @pl.loop(0, 2)
+        def _(d):
+            hidden(lax.rem(z + jnp.where(d == 0, NZ - hop, hop), NZ))
+
+    hidden(z)
+    hidden_pair(1)
+    forward(gu, 2)
+    hidden_pair(2)
+    forward(gu, 3)
+    start(dn, 1)
+    hidden_pair(3)
+    arrive(gu)
+    hidden(lax.rem(z + 4, NZ))
+
+    def down(k, half):
+        left = jnp.concatenate([units[half, o] for o in range(NZ)], axis=1)
+        right = jnp.concatenate([dbuf[o, k * DC : (k + 1) * DC, :] for o in range(NZ)], axis=1)
+        return lax.dot_general(left, right, (((1,), (1,)), ((), ())), preferred_element_type=F32)
+
+    def partial_copy(k):
+        return pltpu.make_async_remote_copy(
+            src_ref=ps.at[k], dst_ref=pr.at[k], send_sem=ps_send.at[k], recv_sem=ps_recv.at[k],
+            device_id=(ep, sib), device_id_type=MESH,
+        )
+
+    def back(k, peer, src):
+        return pltpu.make_async_remote_copy(
+            src_ref=rs.at[k, peer], dst_ref=rb.at[k, src],
+            send_sem=rt_send.at[k, peer], recv_sem=rt_recv.at[k, src],
+            device_id=(peer, tp), device_id_type=MESH,
+        )
+
+    def stage1(k):
+        ps[k] = down(k, 1 - core).astype(BF16)
+        partial_copy(k).start()
+        acc[k] = down(k, core)
+
+    def stage2(k):
+        partial_copy(k).wait_recv()
+        total = acc[k] + pr[k].astype(F32)
+        rs[k] = total.reshape(NEP, CAP, DC).astype(BF16)
+
+        @pl.loop(1, NEP)
+        def _(j):
+            back(k, lax.rem(ep + j, NEP), ep).start()
+
+        rb[k, ep] = rs[k, ep]
+
+    def stage3(k):
+        @pl.loop(1, NEP)
+        def _(j):
+            src = lax.rem(ep + j, NEP)
+            back(k, src, src).wait_recv()
+
+        got = rb[k].astype(F32).reshape(ROWS, DC).astype(BF16)
+        mixed = jnp.dot(comb[0], got, preferred_element_type=F32)
+        mixed = mixed + jnp.dot(comb[1], got, preferred_element_type=F32)
+        out_ref[:, k * DC : (k + 1) * DC] = mixed.astype(BF16)
+
+    first, second = dn[:2], dn[2:]
+    forward(first, 1)
+    forward(first, 2)
+    forward(first, 3)
+    forward(second, 1)
+    arrive(first)
+    stage1(0)
+    forward(second, 2)
+    stage1(1)
+    stage2(0)
+    forward(second, 3)
+    stage2(1)
+    arrive(second[:1])
+    stage1(2)
+    arrive(second[1:])
+    stage1(3)
+    stage2(2)
+    stage2(3)
+    for k in range(NDC):
+        stage3(k)
+
+    for p in gu + dn:
+        for d in (0, 1):
+            for hop in (1, 2, 3, 4):
+                ring(d, hop, p, sent(d, hop)).wait_send()
+
+    @pl.loop(1, NEP)
+    def _(k):
+        peer = lax.rem(ep + k, NEP)
+        dispatch(peer, ep).wait_send()
+        for c in range(NDC):
+            back(c, peer, ep).wait_send()
+
+    to_sib.wait_send()
+    for k in range(NDC):
+        partial_copy(k).wait_send()
+
+
 def expert_half(
     dispatched_group_activity,
     specialist_rmsgain,
@@ -215,39 +457,47 @@
     specialist_widen_maps,
     specialist_shrink_maps,
 ):
-    token_count, model_width = dispatched_group_activity.shape
-    route_count = selected_specialist_ids.shape[1]
-    expert_count = lax.axis_size("ep")
-    slot_count = 3 * route_count * token_count // (2 * expert_count)
-    values = dispatched_group_activity.astype(jnp.float32)
-    scale = lax.rsqrt(jnp.mean(values * values, axis=1, keepdims=True) + 1e-06)
-    normed = (values * scale * specialist_rmsgain.astype(jnp.float32)).astype(jnp.bfloat16)
-    flat_ids = selected_specialist_ids.reshape(-1)
-    one_hot = (flat_ids[:, None] == jnp.arange(expert_count, dtype=jnp.int32)[None, :]).astype(
-        jnp.int32
-    )
-    slot_rank = jnp.sum((jnp.cumsum(one_hot, axis=0) - one_hot) * one_hot, axis=1)
-    slot_place = flat_ids * slot_count + slot_rank
-    owner_token = jnp.arange(token_count * route_count, dtype=jnp.int32) // route_count
-    slot_token = (
-        jnp.full((expert_count * slot_count,), token_count, jnp.int32)
-        .at[slot_place]
-        .set(owner_token)
-    )
-    padded_rows = jnp.concatenate([normed, jnp.zeros((1, model_width), jnp.bfloat16)], axis=0)
-    outgoing = padded_rows[slot_token].reshape(expert_count, slot_count, model_width)
-    arrived = cut_exchange(outgoing, "ep", 2, 0, 0).reshape(expert_count * slot_count, model_width)
-    gate_shard = specialist_switch_maps[0]
-    up_shard = specialist_widen_maps[0]
-    down_shard = specialist_shrink_maps[0]
-    gate_full, up_full, down_full = sent_together((gate_shard, up_shard, down_shard), "tp", 1, 0)
-    result = down_product(expert_units(arrived, gate_full, up_full), down_full)
-    outbound = result.astype(jnp.bfloat16).reshape(expert_count, slot_count, model_width)
-    returned = lax.all_to_all(outbound, "ep", split_axis=0, concat_axis=0, tiled=True).reshape(
-        expert_count * slot_count, model_width
-    )
-    chosen = returned[slot_place].reshape(token_count, route_count, model_width).astype(jnp.float32)
-    return jnp.sum(chosen * selected_specialist_share[:, :, None], axis=1).astype(jnp.bfloat16)
+    meta = jnp.concatenate(
+        [selected_specialist_ids.astype(F32).T, selected_specialist_share.T, jnp.zeros((4, SHARD), F32)], axis=0
+    )
+    vm = pl.BlockSpec(memory_space=pltpu.VMEM)
+    dma = pltpu.SemaphoreType.DMA
+    return pl.pallas_call(
+        expert_kernel,
+        out_shape=jax.ShapeDtypeStruct((SHARD, DM), BF16),
+        in_specs=[vm] * 6,
+        out_specs=vm,
+        scratch_shapes=[
+            pltpu.VMEM((NZ, DM, SHARD), BF16),
+            pltpu.VMEM((NZ, DM, SHARD), BF16),
+            pltpu.VMEM((NZ, DM, SHARD), BF16),
+            pltpu.VMEM((NEP, CAP, DM), BF16),
+            pltpu.VMEM((2, NEP, CAP, DM), BF16),
+            pltpu.VMEM((2, ROWS, DM), BF16),
+            pltpu.VMEM((2, NZ, ROWS, SHARD), BF16),
+            pltpu.VMEM((NDC, ROWS, DC), F32),
+            pltpu.VMEM((NDC, ROWS, DC), BF16),
+            pltpu.VMEM((NDC, ROWS, DC), BF16),
+            pltpu.VMEM((NDC, NEP, CAP, DC), BF16),
+            pltpu.VMEM((NDC, NEP, CAP, DC), BF16),
+            pltpu.VMEM((2, SHARD, ROWS), BF16),
+            dma((2, 4, NG + NDC)), dma((2, 4, NG + NDC)),
+            dma((NEP,)), dma((NEP,)),
+            dma, dma,
+            dma((NDC,)), dma((NDC,)),
+            dma((NDC, NEP)), dma((NDC, NEP)),
+        ],
+        compiler_params=pltpu.CompilerParams(
+            collective_id=0, has_side_effects=True, vmem_limit_bytes=56 * 2**20
+        ),
+    )(
+        dispatched_group_activity,
+        specialist_rmsgain.reshape(1, DM),
+        meta,
+        specialist_switch_maps[0],
+        specialist_widen_maps[0],
+        specialist_shrink_maps[0],
+    )
 
 
 def on_device(

time: 231 us -> 195 us (0.84)
  Pallas kernels: 0 us -> 143 us
  waiting for transfers between devices: 108 us -> 2.51 us
  matrix products: 29.1 us -> 5.42 us
  starting transfers between devices: 39.4 us -> 21.6 us
  other arithmetic: 23.6 us -> 8.94 us
  between operations: 15 us -> 1.5 us
  local copies, waits for them, and re-layouts: 15.4 us -> 11.9 us
    pallas_call x0 -> x1, Pallas kernels: none -> 143 us  [expert_half(): pl.pallas_call(expert_kernel, out_shape=jax.ShapeDtypeStruct((SHARD, DM),...]
    all_gather x1 -> x0, waiting for transfers between devices: 66.8 us -> none  [sent_together(): lax.all_gather(both, axis, axis=dim, tiled=True)]
    all_to_all x3 -> x0, waiting for transfers between devices: 40.8 us -> none  [the longest x1 20.7 us: expert_half(): lax.all_to_all(outbound, 'ep', split_axis=0, concat_axis=0, tiled=True)]
    dot_general x2 -> x0, matrix products: 23.7 us -> none  [the longest x1 15.3 us: down_product(): lax.dot_general(units, down_piece, (((1,), (1,)), ((), ())), preferred_el...]
    all_to_all x3 -> x0, starting transfers between devices: 17 us -> none  [the longest x2 10.3 us: cut_exchange(): lax.all_to_all(section, axis, split_axis=0, concat_axis=0, tiled=True)]
    unnamed x16, other arithmetic: 8.93 us -> 0.36 us
    reduce_sum x3 -> x0, other arithmetic: 4.21 us -> none  [the longest x1 3.93 us: expert_half(): jnp.sum(chosen * selected_specialist_share[:, :, None], axis=1)]
    gather x2 -> x0, local copies, waits for them, and re-layouts: 3.81 us -> none  [the longest x1 2.45 us: expert_half(): padded_rows[slot_token].reshape(expert_count, slot_count, model_width)]
  transfers between devices with their start and end apart: 7 -> 3, of which waited for: 4 -> 1; matrix products, arithmetic and copies ran while one was open for 26% -> 3% of each run, Pallas kernels for 0% -> 73%
where the time goes in v1:
time: 195 us; the launch traced here: 194 us
  Pallas kernels  143 us (73%)
  starting transfers between devices  21.6 us (11%)
  local copies, waits for them, and re-layouts  11.9 us (6%)
  other arithmetic  8.94 us (5%)
  matrix products  5.42 us (3%)
  waiting for transfers between devices  2.51 us (1%)
    pallas_call x1, Pallas kernels, expert_half(): pl.pallas_call(expert_kernel, out_shape=jax.ShapeDtypeStruct((SHARD, DM),...  143 us
    all_to_all x1, starting transfers between devices, mixer_half(): lax.all_to_all(pieces, 'tp', split_axis=1, concat_axis=0, tiled=True)  11.2 us
    all_to_all x1, starting transfers between devices, from_everyone(): return lax.all_to_all(copies, axis, split_axis=0, concat_axis=0, tiled=True)  6.46 us
    ppermute x1, starting transfers between devices, from_behind(): return lax.ppermute(x, axis, pairs)  3.92 us
  transfers between devices with their start and end apart: 3, of which 1 were waited for; matrix products, arithmetic and copies ran while one was open for 3% of the time, Pallas kernels for 73%

profile of v1, /device:TPU:1, one launch (start us, length us, event | category | flops | bytes accessed | tf_op | source)
XLA Modules:
  0.0 194.4 jit_solution(8475407320691076461)
XLA Ops:
  0.6 0.0 copy-start
  0.6 0.8 slice.405
  1.5 3.9 %collective-permute-start = (bf16[64,3]{1,0:T(8,128)(2,1)S(1)}, bf16[64,3]{1,0:T(8,128)(2,1)S(1)}, u32[]{:S(2)}, u32[]{:S(2)}) collective-permute-start(bf16[64,3]{1,0:T(8,128)(2,1)S(1)} %slice.405), channel_id=1, source_target_pairs={{0,16},{16,32},{32,48},{48,64},{64,80},{80,96},{96,112},{112,128},... | collective-permute-start | bytes 1160 | tf_op jit(solution)/shard_map/ppermute | solution.py:73
  5.4 0.8 dynamic-slice_convert_fusion
  6.2 0.8 dynamic-slice_multiply_fusion
  6.9 0.8 add.427
  7.7 0.0 collective-permute-done
  7.7 1.1 maximum_convert_fusion
  8.8 0.5 fusion.16
  9.3 0.0 copy-done
  9.4 0.0 copy-start.4
  9.4 0.3 fusion.7
  9.7 0.3 copy.43
  10.1 0.3 exponential_bitcast_fusion
  10.4 0.9 fusion.44
  11.3 0.1 multiply_multiply_fusion
  11.4 0.0 copy-done.4
  11.4 1.3 fusion.4
  12.7 0.3 copy.45
  13.1 0.3 copy.86
  13.4 0.1 bitcast_add_fusion
  14.9 1.3 pad.101
  16.3 0.7 reshape.85
  17.0 6.5 %all-to-all-start = ((f32[16,1,128]{2,1,0:T(1,128)}), f32[16,1,128]{2,1,0:T(1,128)S(1)}, u32[]{:S(2)}, u32[]{:S(2)}) async-start(f32[16,1,128]{2,1,0:T(1,128)} %reshape.85), calls=%async_computation | async-start | bytes 16384 | tf_op jit(solution)/shard_map/all_to_all | solution.py:28
  23.5 1.3 pad.100
  24.9 0.9 slice_add_fusion.1
  26.1 0.0 copy-start.3
  26.2 0.0 copy-start.2
  26.2 1.0 copy-done.2
  27.2 2.5 %all-to-all-done = f32[16,1,128]{2,1,0:T(1,128)S(1)} async-done(((f32[16,1,128]{2,1,0:T(1,128)}), f32[16,1,128]{2,1,0:T(1,128)S(1)}, u32[]{:S(2)}, u32[]{:S(2)}) %all-to-all-start) | async-done | bytes 8224 | tf_op jit(solution)/shard_map/all_to_all | solution.py:28
  29.7 0.5 broadcast.113
  30.2 0.7 reduce
  30.9 0.1 reshape.86
  31.0 0.1 broadcast_select_fusion.1
  31.4 0.0 copy-start.5
  31.4 0.0 copy-start.6
  31.4 0.0 copy-start.7
  31.4 1.4 add_bitcast_fusion
  32.8 0.6 copy.64
  33.4 0.3 copy.65
  33.7 0.0 copy-done.3
  33.7 0.9 copy_bitcast_fusion.1
  34.6 11.2 %all-to-all-start.1 = ((bf16[64,16,128]{2,0,1:T(8,128)(2,1)}), bf16[64,16,128]{2,0,1:T(8,128)(2,1)S(1)}, u32[]{:S(2)}, u32[]{:S(2)}) async-start(bf16[64,16,128]{2,0,1:T(8,128)(2,1)} %copy_bitcast_fusion.1), calls=%async_computation.1 | async-start | bytes 524288 | tf_op jit(solution)/shard_map/all_to_all | solution.py:196
  45.8 0.0 copy-done.5
  45.9 0.6 reshape.84.gain_ref
  46.5 0.1 pad.120.clone
  46.5 0.0 copy-done.6
  46.5 0.0 copy-done.7
  46.5 0.7 maximum_maximum_fusion.meta_ref
  47.2 142.6 %shard_map.158 = bf16[128,2048]{1,0:T(8,128)(2,1)} custom-call(bf16[128,2048]{1,0:T(8,128)(2,1)} %tok_ref.1, bf16[1,2048]{1,0:T(2,128)(2,1)} %reshape.84.gain_ref, f32[8,128]{1,0:T(8,128)} %maximum_maximum_fusion.meta_ref, bf16[2048,128]{1,0:T(8,128)(2,1)} %bitcast.278, bf16[2048,128]{1,0:T(8,128)(2,1)} %bitcast.279, bf16[2048,128]{1,0:T(8,128)(2,1)} %bitcast.280), custom_call_target="tpu_custom_call" | custom-call | tf_op jit(solution)/shard_map/pallas_call | solution.py:465
  189.8 0.0 copy-start.1
  189.8 0.0 all-to-all-done.1
  189.8 3.8 %convolution_convert_fusion = bf16[128,2048]{1,0:T(8,128)(2,1)} fusion(bf16[1024,128]{1,0:T(8,128)(2,1)S(1)} %bitcast.274, bf16[1024,2048]{1,0:T(8,128)(2,1)} %param.22), kind=kOutput, calls=%fused_computation | convolution fusion | flops 537133056 | bytes 4980736 | tf_op jit(solution)/shard_map/dot_general | solution.py:195
  193.6 0.0 copy-done.1
  193.6 0.8 copy.118
  (148 shorter events, 1.8 us)
Async XLA Ops:
  0.6 8.7 %copy-start = (bf16[16,64,64]{2,1,0:T(8,128)(2,1)S(1)}, bf16[16,64,64]{2,1,0:T(8,128)(2,1)}, u32[]{:S(2)}) copy-start(bf16[16,64,64]{2,1,0:T(8,128)(2,1)} %param.18) | copy-start | bytes 393220
  1.5 6.2 %collective-permute-start = (bf16[64,3]{1,0:T(8,128)(2,1)S(1)}, bf16[64,3]{1,0:T(8,128)(2,1)S(1)}, u32[]{:S(2)}, u32[]{:S(2)}) collective-permute-start(bf16[64,3]{1,0:T(8,128)(2,1)S(1)} %slice.405), channel_id=1, source_target_pairs={{0,16},{16,32},{32,48},{48,64},{64,80},{80,96},{96,112},{112,128},... | collective-permute-start | bytes 1160 | tf_op jit(solution)/shard_map/ppermute | solution.py:73
  9.4 2.1 %copy-start.4 = (f32[2048]{0:T(1024)S(1)}, f32[2048]{0:T(1024)}, u32[]{:S(2)}) copy-start(f32[2048]{0:T(1024)} %param.21) | copy-start | bytes 24580
  17.0 12.7 %all-to-all-start = ((f32[16,1,128]{2,1,0:T(1,128)}), f32[16,1,128]{2,1,0:T(1,128)S(1)}, u32[]{:S(2)}, u32[]{:S(2)}) async-start(f32[16,1,128]{2,1,0:T(1,128)} %reshape.85), calls=%async_computation | async-start | bytes 16384 | tf_op jit(solution)/shard_map/all_to_all | solution.py:28
  26.1 7.6 %copy-start.3 = (bf16[64,2048]{1,0:T(8,128)(2,1)S(1)}, bf16[64,2048]{1,0:T(8,128)(2,1)}, u32[]{:S(2)}) copy-start(bf16[64,2048]{1,0:T(8,128)(2,1)} %param.16) | copy-start | bytes 786436
  26.2 1.0 copy-start.2
  31.4 14.5 %copy-start.5 = (bf16[2048]{0:T(1024)(128)(2,1)S(1)}, bf16[2048]{0:T(1024)(128)(2,1)}, u32[]{:S(2)}) copy-start(bf16[2048]{0:T(1024)(128)(2,1)} %param.24) | copy-start | bytes 12292
  31.4 15.1 %copy-start.6 = (s32[128,2]{0,1:T(2,128)S(1)}, s32[128,2]{0,1:T(2,128)}, u32[]{:S(2)}) copy-start(s32[128,2]{0,1:T(2,128)} %param.25) | copy-start | bytes 3076
  31.4 15.1 %copy-start.7 = (f32[128,2]{0,1:T(2,128)S(1)}, f32[128,2]{0,1:T(2,128)}, u32[]{:S(2)}) copy-start(f32[128,2]{0,1:T(2,128)} %param.26) | copy-start | bytes 3076
  34.6 155.1 %all-to-all-start.1 = ((bf16[64,16,128]{2,0,1:T(8,128)(2,1)}), bf16[64,16,128]{2,0,1:T(8,128)(2,1)S(1)}, u32[]{:S(2)}, u32[]{:S(2)}) async-start(bf16[64,16,128]{2,0,1:T(8,128)(2,1)} %copy_bitcast_fusion.1), calls=%async_computation.1 | async-start | bytes 524288 | tf_op jit(solution)/shard_map/all_to_all | solution.py:196
  189.8 3.8 %copy-start.1 = (bf16[128,2048]{1,0:T(8,128)(2,1)S(1)}, bf16[128,2048]{1,0:T(8,128)(2,1)}, u32[]{:S(2)}) copy-start(bf16[128,2048]{1,0:T(8,128)(2,1)} %shard_map.158) | copy-start | bytes 1572868

commit v2 on v1

v2 whole, which is shorter than its diff:
```python
import jax
import jax.numpy as jnp
from jax import lax
from jax.experimental import pallas as pl
from jax.experimental.pallas import tpu as pltpu
from jax.sharding import PartitionSpec as P

MESH = pl.DeviceIdType.MESH
F32 = jnp.float32
BF16 = jnp.bfloat16
CAP = 24
ROWS = 384
DM = 2048
SHARD = 128
NZ = 8
NEP = 16
NDC = 8
DC = DM // NDC
NG = 4
GROWS = 1024
POS = 2048
HALO = 128
SPAN = 512
CH = 64


def whole_kernel(
    gain_hbm, id_hbm, share_hbm, taps_hbm, rate_hbm, entry_hbm, fading_hbm, spike_hbm,
    src_hbm, gate_hbm, map_hbm, tok_hbm, g_hbm, u_hbm, d_hbm, scan_ref, out_ref,
    gbuf, ubuf, dbuf, snd, xin, xmat, units, acc, ps, pr, rs, rb, comb,
    gain_ref, id_ref, share_ref, taps_ref, rate_ref, entry_ref, fading_ref, spike_ref,
    tok_ref, src_ref, gate_ref, map_ref, state_buf, decay_buf, tot_out, tot_in, mix_out, mix_in,
    ag_send, ag_recv, ds_send, ds_recv, xs_send, xs_recv, ps_send, ps_recv, rt_send, rt_recv,
    scan_out, out_buf, in_sem, out_sem, halo_send, halo_recv, tt_send, tt_recv, mx_send, mx_recv,
):
    ep = lax.axis_index("ep")
    tp = lax.axis_index("tp")
    z = tp // 2
    core = lax.rem(tp, 2)
    sib = z * 2 + (1 - core)
    nbr = (lax.rem(z + 1, NZ) * 2 + core, lax.rem(z + NZ - 1, NZ) * 2 + core)

    loads = [
        pltpu.make_async_copy(src, dst, in_sem.at[i])
        for i, (src, dst) in enumerate(
            (
                (g_hbm, gbuf.at[z]),
                (u_hbm, ubuf.at[z]),
                (tok_hbm, tok_ref),
                (src_hbm, src_ref.at[:, pl.ds(HALO, POS)]),
                (d_hbm, dbuf.at[z]),
                (gate_hbm, gate_ref),
                (map_hbm, map_ref),
                (gain_hbm, gain_ref),
                (id_hbm, id_ref),
                (share_hbm, share_ref),
                (taps_hbm, taps_ref),
                (rate_hbm.at[tp], rate_ref),
                (entry_hbm.at[tp], entry_ref),
                (fading_hbm, fading_ref),
                (spike_hbm, spike_ref),
            )
        )
    ]
    for load in loads:
        load.start()

    bar = pltpu.get_barrier_semaphore()

    @pl.loop(1, NEP)
    def _(k):
        pl.semaphore_signal(bar, inc=1, device_id=(lax.rem(ep + k, NEP), tp), device_id_type=MESH)
        pl.semaphore_signal(bar, inc=1, device_id=(ep, lax.rem(tp + k, NEP)), device_id_type=MESH)

    pl.semaphore_wait(bar, 2 * (NEP - 1))

    def piece(p):
        if p < NG:
            return (gbuf if p < 2 else ubuf, (p % 2) * GROWS, GROWS)
        return dbuf, (p - NG) * DC, DC

    def ring(d, hop, p, origin):
        buf, lo, n = piece(p)
        last = isinstance(hop, int) and hop == 4
        if last:
            n = n // 2
            lo = lo + d * n
        return pltpu.make_async_remote_copy(
            src_ref=buf.at[origin, pl.ds(lo, n)], dst_ref=buf.at[origin, pl.ds(lo, n)],
            send_sem=ag_send.at[d, hop - 1, p], recv_sem=ag_recv.at[d, hop - 1, p],
            device_id=(ep, nbr[d]), device_id_type=MESH,
        )

    def sent(d, hop):
        return lax.rem(z + NZ - (hop - 1), NZ) if d == 0 else lax.rem(z + hop - 1, NZ)

    def came(d, hop):
        return lax.rem(z + NZ - hop, NZ) if d == 0 else lax.rem(z + hop, NZ)

    def start(pieces, hop):
        for p in pieces:
            for d in (0, 1):
                ring(d, hop, p, sent(d, hop)).start()

    def forward(pieces, hop, last=False):
        for p in pieces:
            for d in (0, 1):
                ring(d, hop, p, came(d, hop)).wait_recv()
                nxt = 4 if last else hop + 1
                ring(d, nxt, p, sent(d, nxt)).start()

    def arrive(pieces):
        for p in pieces:
            for d in (0, 1):
                ring(d, 4, p, came(d, 4)).wait_recv()

    gu = list(range(NG))
    dn = list(range(NG, NG + NDC))
    loads[0].wait()
    loads[1].wait()
    start(gu, 1)
    for i in (2, 3, 7, 8, 9, 10, 11, 12, 13, 14):
        loads[i].wait()
    halo = pltpu.make_async_remote_copy(
        src_ref=src_ref.at[:, pl.ds(POS, HALO)], dst_ref=src_ref.at[:, pl.ds(0, HALO)],
        send_sem=halo_send, recv_sem=halo_recv,
        device_id=(lax.rem(ep + 1, NEP), tp), device_id_type=MESH,
    )
    halo.start()

    values = tok_ref[...].astype(F32)
    scale = lax.rsqrt(jnp.mean(values * values, axis=1, keepdims=True) + 1e-06)
    gains = gain_ref[...].astype(F32)
    gain = jnp.concatenate([gains[i : i + 1, :] for i in range(NEP)], axis=1)
    normed = (values * scale * gain).astype(BF16)
    expert_no = lax.broadcasted_iota(jnp.int32, (NEP, SHARD), 0).astype(F32)
    ids = id_ref[...].astype(F32)
    is0 = ids[0:1, :] == expert_no
    is1 = ids[1:2, :] == expert_no
    member = jnp.where(is0 | is1, 1.0, 0.0)
    weight = jnp.where(is0, share_ref[0:1, :], 0.0) + jnp.where(is1, share_ref[1:2, :], 0.0)
    before = (
        lax.broadcasted_iota(jnp.int32, (SHARD, SHARD), 0)
        < lax.broadcasted_iota(jnp.int32, (SHARD, SHARD), 1)
    )
    rank = jnp.dot(
        member.astype(BF16), jnp.where(before, 1.0, 0.0).astype(BF16), preferred_element_type=F32
    )
    place = jnp.where(member > 0.0, rank, -1.0)
    slot_no = lax.broadcasted_iota(jnp.int32, (CAP, SHARD), 0).astype(F32)
    picks, shares = [], []
    for e in range(NEP):
        hit = place[e : e + 1, :] == slot_no
        picks.append(jnp.where(hit, 1.0, 0.0))
        shares.append(jnp.where(hit, weight[e : e + 1, :], 0.0))
    pick = jnp.concatenate(picks, axis=0).astype(BF16)
    share = jnp.concatenate(shares, axis=0).T
    share_hi = share.astype(BF16)
    comb[0] = share_hi
    comb[1] = (share - share_hi.astype(F32)).astype(BF16)
    for k in range(4):
        rows = jnp.dot(pick, normed[:, k * 512 : (k + 1) * 512], preferred_element_type=F32)
        snd[:, :, k * 512 : (k + 1) * 512] = rows.reshape(NEP, CAP, 512).astype(BF16)

    def dispatch(peer, src):
        return pltpu.make_async_remote_copy(
            src_ref=snd.at[peer], dst_ref=xin.at[core, src],
            send_sem=ds_send.at[peer], recv_sem=ds_recv.at[src],
            device_id=(peer, tp), device_id_type=MESH,
        )

    @pl.loop(1, NEP)
    def _(k):
        dispatch(lax.rem(ep + k, NEP), ep).start()

    xin[core, ep] = snd[ep]

    lanes = pl.ds(pl.multiple_of(z * SHARD, SHARD), SHARD)
    taps = jnp.concatenate([taps_ref[:, lanes].astype(F32), jnp.zeros((4, SHARD), F32)], axis=0)
    taps = jnp.concatenate([taps] * 16, axis=0).T
    taps = jnp.where(core == 0, taps[:CH], taps[CH:])
    gates = jnp.concatenate([rate_ref[...].astype(F32).T, entry_ref[...].astype(F32).T], axis=0).astype(BF16)
    speeds = jnp.broadcast_to(fading_ref[pl.ds(z, 1), :], (SHARD, SHARD)).T
    speed = jnp.where(core == 0, speeds[:CH, 0:1], speeds[CH:, 0:1]) * -8.0
    halo.wait_recv()
    place_no = lax.broadcasted_iota(jnp.int32, (CH, SPAN), 1)
    back_no = lax.broadcasted_iota(jnp.int32, (CH, SPAN + HALO), 1)

    def local(k, carry):
        at = pl.multiple_of(k * SPAN, SPAN)
        span = src_ref[:, pl.ds(at, SPAN + HALO)].astype(F32)
        span = jnp.where((back_no < HALO) & (k == 0) & (ep == 0), 0.0, span)
        running = pltpu.roll(span, 3, 1)[:, HALO:] * taps[:, 0:1]
        running = running + pltpu.roll(span, 2, 1)[:, HALO:] * taps[:, 1:2]
        running = running + pltpu.roll(span, 1, 1)[:, HALO:] * taps[:, 2:3]
        running = running + span[:, HALO:] * taps[:, 3:4]
        conv = running.astype(BF16)
        both = jax.nn.sigmoid(jnp.dot(gates, conv, preferred_element_type=F32))
        power = both[:CH] * speed + spike_ref[:, pl.ds(at, SPAN)]
        decay = jnp.exp(power)
        twice = 2.0 * power
        series = 1.0 + twice * (1.0 / 7.0)
        for n in (6.0, 5.0, 4.0, 3.0, 2.0):
            series = 1.0 + twice * (1.0 / n) * series
        left = jnp.where(twice > -0.25, -twice * series, 1.0 - decay * decay)
        drive = jnp.sqrt(left) * both[CH:] * conv.astype(F32)
        step = 1
        while step < SPAN:
            inside = place_no >= step
            drive = drive + decay * jnp.where(inside, pltpu.roll(drive, step, 1), 0.0)
            decay = decay * jnp.where(inside, pltpu.roll(decay, step, 1), 1.0)
            step *= 2
        drive = drive + decay * carry[1]
        decay = decay * carry[0]
        state_buf[:, pl.ds(at, SPAN)] = drive
        decay_buf[:, pl.ds(at, SPAN)] = decay
        return decay[:, SPAN - 1 :], drive[:, SPAN - 1 :]

    ends = lax.fori_loop(0, POS // SPAN, local, (jnp.ones((CH, 1), F32), jnp.zeros((CH, 1), F32)))
    lane = lax.broadcasted_iota(jnp.int32, (CH, SHARD), 1)
    packed = jnp.where(lane == 0, ends[0], jnp.where(lane == 1, ends[1], 0.0))
    tot_out[...] = jnp.concatenate([packed, jnp.zeros((CH, SHARD), F32)], axis=0).T[0:8, :]

    def total(peer, src):
        return pltpu.make_async_remote_copy(
            src_ref=tot_out, dst_ref=tot_in.at[src], send_sem=tt_send.at[peer], recv_sem=tt_recv.at[src],
            device_id=(peer, tp), device_id_type=MESH,
        )

    @pl.loop(1, NEP)
    def _(k):
        total(lax.rem(ep + k, NEP), ep).start()

    tot_in[ep] = tot_out[...]
    forward(gu, 1)

    @pl.loop(1, NEP)
    def _(k):
        src = lax.rem(ep + k, NEP)
        total(src, src).wait_recv()

    entering = jnp.zeros((1, SHARD), F32)
    for src in range(NEP - 1):
        earlier = src < ep
        entering = jnp.where(earlier, tot_in[src, 0:1, :] * entering + tot_in[src, 1:2, :], entering)
    entering = jnp.broadcast_to(entering, (SHARD, SHARD)).T[:CH, 0:1]
    loads[5].wait()

    @pl.loop(0, POS // SPAN)
    def _(k):
        at = pl.multiple_of(k * SPAN, SPAN)
        state = state_buf[:, pl.ds(at, SPAN)] + decay_buf[:, pl.ds(at, SPAN)] * entering
        side = gate_ref[:, pl.ds(at, SPAN)].astype(F32)
        mixed = (state * jax.nn.gelu(side, approximate=True)).astype(BF16)
        for i in range(SPAN // SHARD):
            mix_out[k * (SPAN // SHARD) + i] = mixed[:, i * SHARD : (i + 1) * SHARD]

    def hand(peer, src):
        return pltpu.make_async_remote_copy(
            src_ref=mix_out.at[peer], dst_ref=mix_in.at[src], send_sem=mx_send.at[peer], recv_sem=mx_recv.at[src],
            device_id=(ep, peer), device_id_type=MESH,
        )

    mix_in[tp] = mix_out[tp]

    @pl.loop(1, NEP)
    def _(k):
        src = lax.rem(ep + k, NEP)
        dispatch(src, src).wait_recv()

    to_sib = pltpu.make_async_remote_copy(
        src_ref=xin.at[core], dst_ref=xin.at[core], send_sem=xs_send, recv_sem=xs_recv,
        device_id=(ep, sib), device_id_type=MESH,
    )
    from_sib = pltpu.make_async_remote_copy(
        src_ref=xin.at[1 - core], dst_ref=xin.at[1 - core], send_sem=xs_send, recv_sem=xs_recv,
        device_id=(ep, sib), device_id_type=MESH,
    )
    to_sib.start()
    from_sib.wait_recv()

    @pl.loop(0, 2 * (NEP // 2))
    def _(i):
        half = i // (NEP // 2)
        pair = lax.rem(i, NEP // 2)
        two = xin[half, pl.ds(pair * 2, 2)].astype(F32).reshape(2 * CAP, DM)
        xmat[half, pl.ds(pl.multiple_of(pair * 2 * CAP, 16), 2 * CAP), :] = two.astype(BF16)

    def hidden(origin):
        @pl.loop(0, 2)
        def _(half):
            both = jnp.concatenate([gbuf[origin], ubuf[origin]], axis=1)
            pre = jnp.dot(xmat[half], both, preferred_element_type=F32)
            gate = jnp.minimum(pre[:, :SHARD], 7.0)
            up = jnp.clip(pre[:, SHARD:], -7.0, 7.0)
            units[half, origin] = ((up + 1.0) * gate * jax.nn.sigmoid(1.702 * gate)).astype(BF16)

    def hidden_pair(hop):
        @pl.loop(0, 2)
        def _(d):
            hidden(lax.rem(z + jnp.where(d == 0, NZ - hop, hop), NZ))

    hidden(z)
    hidden_pair(1)
    forward(gu, 2)
    hidden_pair(2)
    forward(gu, 3)
    loads[4].wait()
    start(dn, 1)
    hidden_pair(3)

    arrive(gu)
    hidden(lax.rem(z + 4, NZ))

    def down(k, half):
        left = jnp.concatenate([units[half, o] for o in range(NZ)], axis=1)
        right = jnp.concatenate([dbuf[o, k * DC : (k + 1) * DC, :] for o in range(NZ)], axis=1)
        return lax.dot_general(left, right, (((1,), (1,)), ((), ())), preferred_element_type=F32)

    def partial_copy(k):
        return pltpu.make_async_remote_copy(
            src_ref=ps.at[k], dst_ref=pr.at[k], send_sem=ps_send.at[k], recv_sem=ps_recv.at[k],
            device_id=(ep, sib), device_id_type=MESH,
        )

    def back(k, peer, src):
        return pltpu.make_async_remote_copy(
            src_ref=rs.at[k, peer], dst_ref=rb.at[k, src],
            send_sem=rt_send.at[k, peer], recv_sem=rt_recv.at[k, src],
            device_id=(peer, tp), device_id_type=MESH,
        )

    def stage1(k):
        ps[k] = down(k, 1 - core).astype(BF16)
        partial_copy(k).start()
        acc[k] = down(k, core)

    def stage2(k):
        partial_copy(k).wait_recv()
        total = acc[k] + pr[k].astype(F32)
        rs[k] = total.reshape(NEP, CAP, DC).astype(BF16)

        @pl.loop(1, NEP)
        def _(j):
            back(k, lax.rem(ep + j, NEP), ep).start()

        rb[k, ep] = rs[k, ep]

    def out_copy(k):
        cols = pl.ds(k * DC, DC)
        return pltpu.make_async_copy(out_buf.at[:, cols], out_ref.at[:, cols], out_sem.at[k])

    def stage3(k):
        @pl.loop(1, NEP)
        def _(j):
            src = lax.rem(ep + j, NEP)
            back(k, src, src).wait_recv()

        got = rb[k].astype(F32).reshape(ROWS, DC).astype(BF16)
        mixed = jnp.dot(comb[0], got, preferred_element_type=F32)
        mixed = mixed + jnp.dot(comb[1], got, preferred_element_type=F32)
        out_buf[:, k * DC : (k + 1) * DC] = mixed.astype(BF16)
        out_copy(k).start()

    for i in range(NDC + 6):
        if i < NDC:
            forward(dn[i : i + 1], 1)
        if 0 <= i - 1 < NDC:
            forward(dn[i - 1 : i], 2)
        if 0 <= i - 2 < NDC:
            forward(dn[i - 2 : i - 1], 3)
        if i - 2 == NDC - 1:
            @pl.loop(1, NEP)
            def _(k):
                hand(lax.rem(tp + k, NEP), tp).start()

        if 0 <= i - 4 < NDC:
            stage2(i - 4)
        if 0 <= i - 3 < NDC:
            arrive(dn[i - 3 : i - 2])
            stage1(i - 3)
        if 0 <= i - 6 < NDC - 1:
            stage3(i - 6)
        if i - 6 == NDC - 2:
            loads[6].wait()

            @pl.loop(1, NEP)
            def _(k):
                src = lax.rem(tp + k, NEP)
                hand(src, src).wait_recv()

            hidden_rows = mix_in[...].reshape(NEP * CH, SHARD).astype(F32).T.astype(BF16)

            @pl.loop(0, 4)
            def _(k):
                cols = pl.ds(pl.multiple_of(k * 512, 512), 512)
                scan_out[:, cols] = jnp.dot(hidden_rows, map_ref[:, cols], preferred_element_type=F32).astype(BF16)

            scan_copy = pltpu.make_async_copy(scan_out, scan_ref, out_sem.at[NDC])
            scan_copy.start()
        if i - 6 == NDC - 1:
            stage3(NDC - 1)

    for p in gu + dn:
        for d in (0, 1):
            for hop in (1, 2, 3, 4):
                ring(d, hop, p, sent(d, hop)).wait_send()

    @pl.loop(1, NEP)
    def _(k):
        peer = lax.rem(ep + k, NEP)
        dispatch(peer, ep).wait_send()
        for c in range(NDC):
            back(c, peer, ep).wait_send()

    @pl.loop(1, NEP)
    def _(k):
        total(lax.rem(ep + k, NEP), ep).wait_send()
        hand(lax.rem(tp + k, NEP), tp).wait_send()

    scan_copy.wait()
    for k in range(NDC):
        out_copy(k).wait()
    halo.wait_send()
    to_sib.wait_send()
    for k in range(NDC):
        partial_copy(k).wait_send()


def on_device(
    scan_source_values,
    switch_path_values,
    causal_filter_coefficients,
    scan_switch_blockmap,
    entry_switch_blockmap,
    feature_fading_speeds,
    spike_amount,
    final_linear_map,
    dispatched_group_activity,
    specialist_rmsgain,
    selected_specialist_ids,
    selected_specialist_share,
    specialist_switch_maps,
    specialist_widen_maps,
    specialist_shrink_maps,
):
    hbm = pl.BlockSpec(memory_space=pltpu.HBM)
    dma = pltpu.SemaphoreType.DMA
    result = jax.ShapeDtypeStruct((SHARD, DM), BF16)
    computed = pl.pallas_call(
        whole_kernel,
        out_shape=(result, result),
        in_specs=[hbm] * 15,
        out_specs=(hbm, hbm),
        scratch_shapes=[
            pltpu.VMEM((NZ, DM, SHARD), BF16),
            pltpu.VMEM((NZ, DM, SHARD), BF16),
            pltpu.VMEM((NZ, DM, SHARD), BF16),
            pltpu.VMEM((NEP, CAP, DM), BF16),
            pltpu.VMEM((2, NEP, CAP, DM), BF16),
            pltpu.VMEM((2, ROWS, DM), BF16),
            pltpu.VMEM((2, NZ, ROWS, SHARD), BF16),
            pltpu.VMEM((NDC, ROWS, DC), F32),
            pltpu.VMEM((NDC, ROWS, DC), BF16),
            pltpu.VMEM((NDC, ROWS, DC), BF16),
            pltpu.VMEM((NDC, NEP, CAP, DC), BF16),
            pltpu.VMEM((NDC, NEP, CAP, DC), BF16),
            pltpu.VMEM((2, SHARD, ROWS), BF16),
            pltpu.VMEM((NEP, SHARD), BF16),
            pltpu.VMEM((2, SHARD), jnp.int32),
            pltpu.VMEM((2, SHARD), F32),
            pltpu.VMEM((4, NZ * SHARD), BF16),
            pltpu.VMEM((CH, CH), BF16),
            pltpu.VMEM((CH, CH), BF16),
            pltpu.VMEM((NZ, SHARD), F32),
            pltpu.VMEM((1, POS), F32),
            pltpu.VMEM((SHARD, DM), BF16),
            pltpu.VMEM((CH, HALO + POS), BF16),
            pltpu.VMEM((CH, POS), BF16),
            pltpu.VMEM((NEP * CH, DM), BF16),
            pltpu.VMEM((CH, POS), F32),
            pltpu.VMEM((CH, POS), F32),
            pltpu.VMEM((8, SHARD), F32),
            pltpu.VMEM((NEP, 8, SHARD), F32),
            pltpu.VMEM((NEP, CH, SHARD), BF16),
            pltpu.VMEM((NEP, CH, SHARD), BF16),
            dma((2, 4, NG + NDC)), dma((2, 4, NG + NDC)),
            dma((NEP,)), dma((NEP,)),
            dma, dma,
            dma((NDC,)), dma((NDC,)),
            dma((NDC, NEP)), dma((NDC, NEP)),
            pltpu.VMEM((SHARD, DM), BF16),
            pltpu.VMEM((SHARD, DM), BF16),
            dma((15,)), dma((NDC + 1,)), dma, dma,
            dma((NEP,)), dma((NEP,)),
            dma((NEP,)), dma((NEP,)),
        ],
        compiler_params=pltpu.CompilerParams(
            collective_id=0, has_side_effects=True, vmem_limit_bytes=62 * 2**20
        ),
    )(
        specialist_rmsgain.reshape(NEP, SHARD),
        selected_specialist_ids.T,
        selected_specialist_share.T,
        causal_filter_coefficients.T,
        scan_switch_blockmap,
        entry_switch_blockmap,
        feature_fading_speeds.reshape(8, SHARD),
        spike_amount.reshape(1, POS),
        scan_source_values,
        switch_path_values,
        final_linear_map,
        dispatched_group_activity,
        specialist_switch_maps[0],
        specialist_widen_maps[0],
        specialist_shrink_maps[0],
    )
    return pl.pallas_call(
        handover_kernel,
        out_shape=(result, result),
        in_specs=[hbm] * 2,
        out_specs=(hbm, hbm),
        scratch_shapes=[pltpu.VMEM((4, SHARD // 2, DM), BF16), dma((4,)), dma((4,))],
    )(*computed)


def handover_kernel(scan_in, moe_in, scan_ref, moe_ref, stage, in_sem, out_sem):
    half = SHARD // 2
    parts = [(a, b, pl.ds(h * half, half)) for a, b in ((scan_in, scan_ref), (moe_in, moe_ref)) for h in (0, 1)]
    ins = [pltpu.make_async_copy(a.at[r], stage.at[i], in_sem.at[i]) for i, (a, b, r) in enumerate(parts)]
    outs = [pltpu.make_async_copy(stage.at[i], b.at[r], out_sem.at[i]) for i, (a, b, r) in enumerate(parts)]
    for copy in ins:
        copy.start()
    for i in range(4):
        ins[i].wait()
        outs[i].start()
    for copy in outs:
        copy.wait()


def solution(mesh):
    in_specs = (
        P("tp", "ep"),
        P("tp", "ep"),
        P(),
        P(),
        P(),
        P(),
        P("ep"),
        P(),
        P(("ep", "tp"), None),
        P(),
        P(("ep", "tp"), None),
        P(("ep", "tp"), None),
        P("ep", None, "tp"),
        P("ep", None, "tp"),
        P("ep", None, "tp"),
    )
    out_specs = (P(("ep", "tp"), None), P(("ep", "tp"), None))
    return jax.shard_map(
        on_device, mesh=mesh, in_specs=in_specs, out_specs=out_specs, check_vma=False
    )
```

time: 195 us -> 151 us (0.77)
  starting transfers between devices: 21.6 us -> 0 us
  local copies, waits for them, and re-layouts: 11.9 us -> 0 us
  other arithmetic: 8.94 us -> 0 us
  Pallas kernels: 143 us -> 151 us
  matrix products: 5.42 us -> 0 us
  waiting for transfers between devices: 2.51 us -> 0 us
    all_to_all x2 -> x0, starting transfers between devices: 17.7 us -> none  [the longest x1 11.2 us: mixer_half(): lax.all_to_all(pieces, 'tp', split_axis=1, concat_axis=0, tiled=True)]
    pallas_call x1 -> x2, Pallas kernels: 143 us -> 151 us  [the longest x1 149 us: on_device(): pl.pallas_call(whole_kernel, out_shape=(result, result), in_specs=[hbm] *...]
    dot_general x3 -> x0, matrix products: 5.42 us -> none  [the longest x1 3.78 us: mixer_half(): lax.dot_general(lax.all_to_all(pieces, 'tp', split_axis=1, concat_axis=0,...]
    ppermute x1 -> x0, starting transfers between devices: 3.92 us -> none  [from_behind(): return lax.ppermute(x, axis, pairs)]
    pad x24 -> x0, local copies, waits for them, and re-layouts: 2.71 us -> none  [segment_recurrence(): lax.associative_scan(combine_pairs, (run_decay, run_state), axis=1)]
    unnamed x22 -> x0, local copies, waits for them, and re-layouts: 2.62 us -> none
    slice x59 -> x0, local copies, waits for them, and re-layouts: 2.62 us -> none  [the longest x1 0.9 us: segment_recurrence(): run_state = decay_split[:, offset] * run_state + drive_split[:, offset]]
    all_to_all x2 -> x0, waiting for transfers between devices: 2.51 us -> none  [the longest x1 2.5 us: from_everyone(): return lax.all_to_all(copies, axis, split_axis=0, concat_axis=0, tiled=True)]
  transfers between devices with their start and end apart: 3 -> 0, of which waited for: 1 -> 0; matrix products, arithmetic and copies ran while one was open for 3% -> 0% of each run, Pallas kernels for 73% -> 0%
where the time goes in v2:
time: 151 us
  Pallas kernels  151 us (100%)
    pallas_call x1, Pallas kernels, on_device(): pl.pallas_call(whole_kernel, out_shape=(result, result), in_specs=[hbm] *...  149 us

profile of v2, /device:TPU:1, one launch (start us, length us, event | category | flops | bytes accessed | tf_op | source)
XLA Modules:
  0.0 151.3 jit_solution(2040415446066485358)
XLA Ops:
  0.6 148.7 %shard_map.158 = (bf16[128,2048]{1,0:T(8,128)(2,1)}, bf16[128,2048]{1,0:T(8,128)(2,1)}) custom-call(bf16[16,128]{1,0:T(8,128)(2,1)} %bitcast.14, s32[2,128]{1,0:T(2,128)} %bitcast.16, f32[2,128]{1,0:T(2,128)} %bitcast.17, bf16[4,1024]{1,0:T(4,128)(2,1)} %bitcast.12, bf16[16,64,64]{2,1,0:T(8,128)(2,1)} %rate_hbm.1, bf16[16,64,64]{2,1,0:T(8,128)(2,1)} %entry_hbm.1, ...), custom_call_target="tpu_custom_call" | custom-call | tf_op jit(solution)/shard_map/pallas_call | solution.py:450
  149.3 2.0 %shard_map.159 = (bf16[128,2048]{1,0:T(8,128)(2,1)}, bf16[128,2048]{1,0:T(8,128)(2,1)}) custom-call(bf16[128,2048]{1,0:T(8,128)(2,1)} %get-tuple-element.4.scan_in, bf16[128,2048]{1,0:T(8,128)(2,1)} %get-tuple-element.5.moe_in), custom_call_target="tpu_custom_call" | custom-call | tf_op jit(solution)/shard_map/pallas_call | solution.py:518

commit v3 on v2

--- a/solution.py
+++ b/solution.py
@@ -14,8 +14,8 @@
 SHARD = 128
 NZ = 8
 NEP = 16
-NDC = 8
-DC = DM // NDC
+DCS = (512, 512, 256, 256, 256, 256)
+NDC = len(DCS)
 NG = 4
 GROWS = 1024
 POS = 2048
@@ -77,7 +77,7 @@
     def piece(p):
         if p < NG:
             return (gbuf if p < 2 else ubuf, (p % 2) * GROWS, GROWS)
-        return dbuf, (p - NG) * DC, DC
+        return dbuf, sum(DCS[: p - NG]), DCS[p - NG]
 
     def ring(d, hop, p, origin):
         buf, lo, n = piece(p)
@@ -313,41 +313,42 @@
     hidden(lax.rem(z + 4, NZ))
 
     def down(k, half):
+        lo = sum(DCS[:k])
         left = jnp.concatenate([units[half, o] for o in range(NZ)], axis=1)
-        right = jnp.concatenate([dbuf[o, k * DC : (k + 1) * DC, :] for o in range(NZ)], axis=1)
+        right = jnp.concatenate([dbuf[o, lo : lo + DCS[k], :] for o in range(NZ)], axis=1)
         return lax.dot_general(left, right, (((1,), (1,)), ((), ())), preferred_element_type=F32)
 
     def partial_copy(k):
         return pltpu.make_async_remote_copy(
-            src_ref=ps.at[k], dst_ref=pr.at[k], send_sem=ps_send.at[k], recv_sem=ps_recv.at[k],
+            src_ref=ps[k], dst_ref=pr[k], send_sem=ps_send.at[k], recv_sem=ps_recv.at[k],
             device_id=(ep, sib), device_id_type=MESH,
         )
 
     def back(k, peer, src):
         return pltpu.make_async_remote_copy(
-            src_ref=rs.at[k, peer], dst_ref=rb.at[k, src],
+            src_ref=rs[k].at[peer], dst_ref=rb[k].at[src],
             send_sem=rt_send.at[k, peer], recv_sem=rt_recv.at[k, src],
             device_id=(peer, tp), device_id_type=MESH,
         )
 
     def stage1(k):
-        ps[k] = down(k, 1 - core).astype(BF16)
+        ps[k][...] = down(k, 1 - core).astype(BF16)
         partial_copy(k).start()
-        acc[k] = down(k, core)
+        acc[k][...] = down(k, core)
 
     def stage2(k):
         partial_copy(k).wait_recv()
-        total = acc[k] + pr[k].astype(F32)
-        rs[k] = total.reshape(NEP, CAP, DC).astype(BF16)
+        total = acc[k][...] + pr[k][...].astype(F32)
+        rs[k][...] = total.reshape(NEP, CAP, DCS[k]).astype(BF16)
 
         @pl.loop(1, NEP)
         def _(j):
             back(k, lax.rem(ep + j, NEP), ep).start()
 
-        rb[k, ep] = rs[k, ep]
+        rb[k][ep] = rs[k][ep]
 
     def out_copy(k):
-        cols = pl.ds(k * DC, DC)
+        cols = pl.ds(sum(DCS[:k]), DCS[k])
         return pltpu.make_async_copy(out_buf.at[:, cols], out_ref.at[:, cols], out_sem.at[k])
 
     def stage3(k):
@@ -356,10 +357,10 @@
             src = lax.rem(ep + j, NEP)
             back(k, src, src).wait_recv()
 
-        got = rb[k].astype(F32).reshape(ROWS, DC).astype(BF16)
+        got = rb[k][...].astype(F32).reshape(ROWS, DCS[k]).astype(BF16)
         mixed = jnp.dot(comb[0], got, preferred_element_type=F32)
         mixed = mixed + jnp.dot(comb[1], got, preferred_element_type=F32)
-        out_buf[:, k * DC : (k + 1) * DC] = mixed.astype(BF16)
+        out_buf[:, sum(DCS[:k]) : sum(DCS[: k + 1])] = mixed.astype(BF16)
         out_copy(k).start()
 
     for i in range(NDC + 6):
@@ -460,11 +461,11 @@
             pltpu.VMEM((2, NEP, CAP, DM), BF16),
             pltpu.VMEM((2, ROWS, DM), BF16),
             pltpu.VMEM((2, NZ, ROWS, SHARD), BF16),
-            pltpu.VMEM((NDC, ROWS, DC), F32),
-            pltpu.VMEM((NDC, ROWS, DC), BF16),
-            pltpu.VMEM((NDC, ROWS, DC), BF16),
-            pltpu.VMEM((NDC, NEP, CAP, DC), BF16),
-            pltpu.VMEM((NDC, NEP, CAP, DC), BF16),
+            tuple(pltpu.VMEM((ROWS, w), F32) for w in DCS),
+            tuple(pltpu.VMEM((ROWS, w), BF16) for w in DCS),
+            tuple(pltpu.VMEM((ROWS, w), BF16) for w in DCS),
+            tuple(pltpu.VMEM((NEP, CAP, w), BF16) for w in DCS),
+            tuple(pltpu.VMEM((NEP, CAP, w), BF16) for w in DCS),
             pltpu.VMEM((2, SHARD, ROWS), BF16),
             pltpu.VMEM((NEP, SHARD), BF16),
             pltpu.VMEM((2, SHARD), jnp.int32),

time: 151 us -> 150 us (level)
  Pallas kernels: 151 us -> 149 us
where the time goes in v3:
time: 150 us
  Pallas kernels  149 us (99%)
    pallas_call x1, Pallas kernels, on_device(): pl.pallas_call(whole_kernel, out_shape=(result, result), in_specs=[hbm] *...  147 us

profile of v3, /device:TPU:1, one launch (start us, length us, event | category | flops | bytes accessed | tf_op | source)
XLA Modules:
  0.0 150.0 jit_solution(11153687102243972701)
XLA Ops:
  0.6 147.3 %shard_map.158 = (bf16[128,2048]{1,0:T(8,128)(2,1)}, bf16[128,2048]{1,0:T(8,128)(2,1)}) custom-call(bf16[16,128]{1,0:T(8,128)(2,1)} %bitcast.14, s32[2,128]{1,0:T(2,128)} %bitcast.16, f32[2,128]{1,0:T(2,128)} %bitcast.17, bf16[4,1024]{1,0:T(4,128)(2,1)} %bitcast.12, bf16[16,64,64]{2,1,0:T(8,128)(2,1)} %rate_hbm.1, bf16[16,64,64]{2,1,0:T(8,128)(2,1)} %entry_hbm.1, ...), custom_call_target="tpu_custom_call" | custom-call | tf_op jit(solution)/shard_map/pallas_call | solution.py:451
  148.0 2.0 %shard_map.159 = (bf16[128,2048]{1,0:T(8,128)(2,1)}, bf16[128,2048]{1,0:T(8,128)(2,1)}) custom-call(bf16[128,2048]{1,0:T(8,128)(2,1)} %get-tuple-element.4.scan_in, bf16[128,2048]{1,0:T(8,128)(2,1)} %get-tuple-element.5.moe_in), custom_call_target="tpu_custom_call" | custom-call | tf_op jit(solution)/shard_map/pallas_call | solution.py:519
